TPU v7x, 32 devices: a whole 2x2x4 slice. The times are simulated.
32 devices in a mesh: ep: 8 (over z, core), tp: 4 (over y, x).
Axes of the slice: x: 2, y: 2, z: 4, core: 2. Of those that a mesh axis runs over, the one named last changes fastest.
Arguments:
- tokens: bfloat16 [384, 2048], P('ep', 'tp'), may hold values from -64 to 64
- mix_gain: float32 [2048], replicated, may hold values from 0.1 to 1.9
- w_gate_z: bfloat16 [2048, 2048], P(None, 'tp'), may hold values from -0.125 to 0.125
- w_value_x: bfloat16 [2048, 2048], P(None, 'tp'), may hold values from -0.125 to 0.125
- w_key_b: bfloat16 [2048, 256], replicated, may hold values from -0.125 to 0.125
- w_query_c: bfloat16 [2048, 256], replicated, may hold values from -0.125 to 0.125
- w_step: bfloat16 [2048, 32], replicated, may hold values from -0.125 to 0.125
- step_bias: float32 [32], replicated, may hold values from -2 to 1
- decay_log: float32 [32], replicated, may hold values from -3 to 1.4
- skip_gain: float32 [32], replicated, may hold values from 0.1 to 1.9
- conv_x_weight: bfloat16 [4, 2048], P(None, 'tp'), may hold values from -3 to 3
- conv_b_weight: bfloat16 [4, 256], replicated, may hold values from -3 to 3
- conv_c_weight: bfloat16 [4, 256], replicated, may hold values from -3 to 3
- window_x: bfloat16 [384, 3, 2048], P('ep', None, 'tp'), may hold values from -6 to 6
- window_b: bfloat16 [384, 3, 256], P('ep'), may hold values from -6 to 6
- window_c: bfloat16 [384, 3, 256], P('ep'), may hold values from -6 to 6
- ssm_state: float32 [384, 32, 64, 128], P('ep', 'tp'), may hold values from -2 to 2
- head_gain: float32 [2048], P('tp'), may hold values from 0.1 to 1.9
- w_out: bfloat16 [2048, 2048], P('tp'), may hold values from -0.1875 to 0.1875
- ffn_gain: float32 [2048], replicated, may hold values from 0.1 to 1.9
- route_ids: int32 [384, 2], P('ep'), may hold values from 0 to 31, all different within a row; in each aligned block of 48 rows (0 to 47, 48 to 95, ...) at most 5 rows name the same one
- route_weights: float32 [384, 2], P('ep'), may hold values from 0.05 to 1
- expert_gate: bfloat16 [8, 2048, 4096], P('ep', None, 'tp'), may hold values from -0.125 to 0.125
- expert_up: bfloat16 [8, 2048, 4096], P('ep', None, 'tp'), may hold values from -0.125 to 0.125
- expert_down: bfloat16 [8, 4096, 2048], P('ep', 'tp'), may hold values from -0.25 to 0.25
Outputs:
- layer_out: bfloat16 [384, 2048], P('ep', 'tp')
Inputs may be any that keep to these rules, and one draw needn't show every extreme that they name: `route_ids`: each row names 2 different experts. Within the rows of one index of ep (aligned blocks of 48 rows) no expert is named by more than 5 rows, a bound that some block reaches.
All inputs are finite; a program needn't handle non-finite values.
Results may differ from a plain program's by a relative error of at most 0.009.
Values may be sent and summed in bfloat16 or wider, within the bound.
A program may use at most 64 MiB of HBM per device.

v0:
```python
import functools

import jax
import jax.numpy as jnp
from jax import lax
from jax.experimental import pallas as pl
from jax.experimental.pallas import tpu as pltpu
from jax.sharding import PartitionSpec as P

HEADS = 32
HEAD_DIM = 64
STATE = 128
GROUPS = 2
EXP_IN = 4


norm_epsilon = 1e-06


def row_norm(arr_values, norm_gain):
    widened = arr_values.astype(jnp.float32)
    return (
        widened
        * lax.rsqrt(jnp.mean(widened * widened, axis=-1, keepdims=True) + norm_epsilon)
        * norm_gain
    )


def short_conv(window, fresh_row, weight):
    conv_taps = weight.astype(jnp.float32)
    summed = (
        jnp.sum(window.astype(jnp.float32) * conv_taps[:-1][None], axis=1)
        + fresh_row * conv_taps[-1]
    )
    return jax.nn.silu(summed)


def product(left, right):
    return jnp.dot(left, right, preferred_element_type=jnp.float32)


def local_plain(
    tokens,
    mix_gain,
    w_gate_z,
    w_value_x,
    w_key_b,
    w_query_c,
    w_step,
    step_bias,
    decay_log,
    skip_gain,
    conv_x_weight,
    conv_b_weight,
    conv_c_weight,
    window_x,
    window_b,
    window_c,
    ssm_state,
    head_gain,
    w_out,
    ffn_gain,
    route_ids,
    route_weights,
    expert_gate,
    expert_up,
    expert_down,
):
    tp_index = lax.axis_index("tp")
    tp_count = lax.axis_size("tp")
    ep_count = lax.axis_size("ep")
    seq_count = tokens.shape[0]
    gathered = lax.all_gather(tokens, "tp", axis=1, tiled=True)
    normed = row_norm(gathered, mix_gain).astype(jnp.bfloat16)
    local_width = w_gate_z.shape[1]
    head_count = local_width // HEAD_DIM
    first_head = tp_index * head_count
    group_start = first_head // (HEADS // GROUPS) * STATE
    gate_z = product(normed, w_gate_z)
    values = short_conv(window_x, product(normed, w_value_x), conv_x_weight)
    key_b = short_conv(
        lax.dynamic_slice_in_dim(window_b, group_start, STATE, 2),
        product(normed, lax.dynamic_slice_in_dim(w_key_b, group_start, STATE, 1)),
        lax.dynamic_slice_in_dim(conv_b_weight, group_start, STATE, 1),
    )
    query_c = short_conv(
        lax.dynamic_slice_in_dim(window_c, group_start, STATE, 2),
        product(normed, lax.dynamic_slice_in_dim(w_query_c, group_start, STATE, 1)),
        lax.dynamic_slice_in_dim(conv_c_weight, group_start, STATE, 1),
    )
    step_all = product(normed, w_step) + step_bias
    step_size = jax.nn.softplus(lax.dynamic_slice_in_dim(step_all, first_head, head_count, 1))
    rate_heads = jnp.exp(lax.dynamic_slice_in_dim(decay_log, first_head, head_count, 0))
    skip_heads = lax.dynamic_slice_in_dim(skip_gain, first_head, head_count, 0)
    decay_heads = jnp.exp(-step_size * rate_heads)
    value_heads = values.reshape(seq_count, head_count, HEAD_DIM)
    new_state = (
        decay_heads[:, :, None, None] * ssm_state
        + (step_size[:, :, None] * value_heads)[..., None] * key_b[:, None, None, :]
    )
    read_out = jnp.einsum("shpn,sn->shp", new_state, query_c, precision=lax.Precision.HIGHEST)
    read_out = read_out + skip_heads[None, :, None] * value_heads
    gated = read_out * jax.nn.silu(gate_z.reshape(seq_count, head_count, HEAD_DIM))
    gated = gated * lax.rsqrt(jnp.mean(gated * gated, axis=-1, keepdims=True) + norm_epsilon)
    mixed_heads = (
        (gated * head_gain.reshape(head_count, HEAD_DIM))
        .reshape(seq_count, local_width)
        .astype(jnp.bfloat16)
    )
    partial_value = product(mixed_heads, w_out)
    share_mix = lax.psum_scatter(partial_value, "tp", scatter_dimension=1, tiled=True)
    residual_own = (tokens.astype(jnp.float32) + share_mix).astype(jnp.bfloat16)
    residual_full = lax.all_gather(residual_own, "tp", axis=1, tiled=True)
    ffn_in = row_norm(residual_full, ffn_gain).astype(jnp.bfloat16)
    top_count = route_ids.shape[1]
    expert_count = EXP_IN * ep_count
    capacity = max(2, (3 * seq_count * top_count + 2 * expert_count - 1) // (2 * expert_count))
    sub_index = tp_index // (tp_count // EXP_IN)
    target_set = route_ids // EXP_IN
    hit_mask = route_ids % EXP_IN == sub_index
    set_grid = jnp.arange(ep_count, dtype=jnp.int32)
    set_onehot = (hit_mask[:, :, None] & (target_set[:, :, None] == set_grid)).astype(jnp.int32)
    set_onehot = set_onehot.reshape(seq_count * top_count, ep_count)
    earlier = jnp.cumsum(set_onehot, axis=0) - set_onehot
    slot_rank = jnp.sum(earlier * set_onehot, axis=1).reshape(seq_count, top_count)
    slot_index = jnp.where(hit_mask, target_set * capacity + slot_rank, -1)
    slot_grid = jnp.arange(ep_count * capacity, dtype=jnp.int32)
    slot_match = slot_index[:, :, None] == slot_grid
    placed = jnp.any(slot_match, axis=1).astype(jnp.bfloat16)
    outgoing = jnp.einsum("sj,sd->jd", placed, ffn_in, preferred_element_type=jnp.float32)
    outgoing = outgoing.astype(jnp.bfloat16).reshape(ep_count, capacity, ffn_in.shape[1])
    route_share = route_weights / jnp.sum(route_weights, axis=1, keepdims=True)
    combine_weight = jnp.sum(jnp.where(slot_match, route_share[:, :, None], 0.0), axis=1)
    arrived = lax.all_to_all(outgoing, "ep", split_axis=0, concat_axis=0, tiled=True)
    source_count, slot_count, row_width = arrived.shape
    flat_rows = arrived.reshape(source_count * slot_count, row_width)
    gate_part = product(flat_rows, expert_gate[0])
    up_part = product(flat_rows, expert_up[0])
    hidden = (jax.nn.silu(gate_part) * up_part).astype(jnp.bfloat16)
    expert_out = product(hidden, expert_down[0]).reshape(source_count, slot_count, row_width)
    returned = lax.all_to_all(
        expert_out.astype(jnp.bfloat16), "ep", split_axis=0, concat_axis=0, tiled=True
    ).astype(expert_out.dtype)
    moe_part = jnp.dot(
        combine_weight,
        returned.reshape(ep_count * capacity, -1),
        precision=lax.Precision.HIGHEST,
        preferred_element_type=jnp.float32,
    )
    moe_share = lax.psum_scatter(
        moe_part.astype(jnp.bfloat16), "tp", scatter_dimension=1, tiled=True
    ).astype(jnp.float32)
    return (residual_own.astype(jnp.float32) + moe_share).astype(jnp.bfloat16)


MESH = pl.DeviceIdType.MESH
HIGH = lax.Precision.HIGHEST
BF = jnp.bfloat16
F32 = jnp.float32
SLOT_ROWS = 8
TILE = 256


def silu(v):
    return v / (1.0 + jnp.exp(-v))


def dot32(left, right, precision=None):
    return jnp.dot(left, right, preferred_element_type=F32, precision=precision)


def layer_entry(n_ep, n_tp, n_small, *refs):
    held, small_sem = refs[-1 - n_small : -1], refs[-1]
    fetches = [
        pltpu.make_async_copy(refs[at], held[at], small_sem.at[at]) for at in range(n_small)
    ]
    layer_kernel(n_ep, n_tp, fetches, *held, *refs[n_small : -1 - n_small])


def layer_kernel(
    n_ep,
    n_tp,
    fetches,
    tokens,
    mix_gain,
    step_bias,
    decay_log,
    skip_gain,
    conv_x,
    conv_b,
    conv_c,
    window_x,
    window_b,
    window_c,
    head_gain,
    ffn_gain,
    ids_t,
    scores_t,
    hbm_gate_z,
    hbm_value_x,
    hbm_key_b,
    hbm_query_c,
    hbm_step,
    hbm_state,
    hbm_out,
    hbm_exp_gate,
    hbm_exp_up,
    hbm_exp_down,
    out,
    w_gate_z,
    w_value_x,
    w_key_b,
    w_query_c,
    w_step,
    state,
    w_out,
    exp_gate,
    exp_up,
    exp_down,
    gathered,
    normed,
    gate_z,
    values,
    queries,
    state_read,
    mix_send,
    mix_recv,
    row_send,
    row_recv,
    rows_in,
    hidden,
    back_send,
    back_recv,
    load_sem,
    state_sem,
    tok_send_sem,
    tok_recv_sem,
    mix_send_sem,
    mix_recv_sem,
    row_send_sem,
    row_recv_sem,
    back_send_sem,
    back_recv_sem,
):
    me_e = lax.axis_index("ep")
    me_t = lax.axis_index("tp")
    seqs, width = tokens.shape
    features = width * n_tp
    heads_here = width // HEAD_DIM
    first_head = me_t * heads_here
    group_start = pl.multiple_of(first_head // (HEADS // GROUPS) * STATE, STATE)
    group_cols = pl.ds(group_start, STATE)
    n_all = n_ep * n_tp

    def load(source, target, index):
        return pltpu.make_async_copy(source, target, load_sem.at[index])

    load_key = load(hbm_key_b.at[:, group_cols], w_key_b, 0)
    load_query = load(hbm_query_c.at[:, group_cols], w_query_c, 1)
    load_step = load(hbm_step, w_step, 2)
    load_value = load(hbm_value_x, w_value_x, 3)
    load_gate = load(hbm_gate_z, w_gate_z, 4)
    load_out = load(hbm_out, w_out, 5)
    load_exp_gate = load(hbm_exp_gate, exp_gate, 6)
    load_exp_up = load(hbm_exp_up, exp_up, 7)
    load_exp_down = load(hbm_exp_down, exp_down, 8)

    def load_state(block):
        rows = pl.ds(block * 8, 8)
        return pltpu.make_async_copy(hbm_state.at[rows], state.at[rows], state_sem.at[block])

    barrier = pltpu.get_barrier_semaphore()

    def greet(offset, carry):
        other = lax.rem(me_e * n_tp + me_t + offset, n_all)
        pl.semaphore_signal(
            barrier, inc=1, device_id=(other // n_tp, lax.rem(other, n_tp)), device_id_type=MESH
        )
        return carry

    for each in fetches:
        each.start()
    lax.fori_loop(1, n_all, greet, 0)
    for each in (load_query, load_key, load_step, load_value, load_gate):
        each.start()
    for block in range(seqs // 8):
        load_state(block).start()
    for each in (load_out, load_exp_gate, load_exp_up, load_exp_down):
        each.start()
    for each in fetches:
        each.wait()
    gathered[me_t] = tokens[...]
    pl.semaphore_wait(barrier, n_all - 1)

    def token_copy(step):
        return pltpu.make_async_remote_copy(
            src_ref=tokens,
            dst_ref=gathered.at[me_t],
            send_sem=tok_send_sem.at[step],
            recv_sem=tok_recv_sem.at[me_t],
            device_id=(me_e, lax.rem(me_t + step, n_tp)),
            device_id_type=MESH,
        )

    def token_arrival(step):
        source = lax.rem(me_t + step, n_tp)
        return pltpu.make_async_remote_copy(
            src_ref=tokens,
            dst_ref=gathered.at[source],
            send_sem=tok_send_sem.at[step],
            recv_sem=tok_recv_sem.at[source],
            device_id=(me_e, source),
            device_id_type=MESH,
        )

    for step in range(1, n_tp):
        token_copy(step).start()

    n_exp = n_ep * EXP_IN
    n_slots = n_exp * SLOT_ROWS
    row_at = lax.broadcasted_iota(jnp.int32, (seqs, seqs), 0)
    col_at = lax.broadcasted_iota(jnp.int32, (seqs, seqs), 1)

    def stood_up(row):
        return jnp.sum(jnp.where(row_at == col_at, row, 0.0), axis=1, keepdims=True)

    id0 = stood_up(ids_t[0:1, :].astype(F32)).astype(jnp.int32)
    id1 = stood_up(ids_t[1:2, :].astype(F32)).astype(jnp.int32)
    lane_exp = lax.broadcasted_iota(jnp.int32, (seqs, n_exp), 1)
    hit0 = jnp.where(id0 == lane_exp, 1.0, 0.0)
    hit1 = jnp.where(id1 == lane_exp, 1.0, 0.0)
    lower = jnp.where(row_at > col_at, 1.0, 0.0).astype(BF)
    upper = jnp.where(row_at < col_at, 1.0, 0.0).astype(BF)
    before = dot32(lower, (hit0 + hit1).astype(BF))
    slot0 = id0 * SLOT_ROWS + jnp.sum(before * hit0, axis=1, keepdims=True).astype(jnp.int32)
    slot1 = id1 * SLOT_ROWS + jnp.sum(before * hit1, axis=1, keepdims=True).astype(jnp.int32)
    lane_slot = lax.broadcasted_iota(jnp.int32, (seqs, n_slots), 1)
    score0, score1 = stood_up(scores_t[0:1, :]), stood_up(scores_t[1:2, :])
    total = score0 + score1
    combine = jnp.where(slot0 == lane_slot, score0 / total, 0.0) + jnp.where(
        slot1 == lane_slot, score1 / total, 0.0
    )
    combine_high = combine.astype(BF)
    combine_low = (combine - combine_high.astype(F32)).astype(BF)

    idt0, idt1 = ids_t[0:1, :], ids_t[1:2, :]
    sub_exp = lax.broadcasted_iota(jnp.int32, (n_exp, seqs), 0)
    hitt0 = jnp.where(idt0 == sub_exp, 1.0, 0.0)
    hitt1 = jnp.where(idt1 == sub_exp, 1.0, 0.0)
    before_t = dot32((hitt0 + hitt1).astype(BF), upper)
    slott0 = idt0 * SLOT_ROWS + jnp.sum(before_t * hitt0, axis=0, keepdims=True).astype(jnp.int32)
    slott1 = idt1 * SLOT_ROWS + jnp.sum(before_t * hitt1, axis=0, keepdims=True).astype(jnp.int32)
    sub_slot = lax.broadcasted_iota(jnp.int32, (n_slots, seqs), 0)
    placed = jnp.where((slott0 == sub_slot) | (slott1 == sub_slot), 1.0, 0.0).astype(BF)

    def window_sum(window, taps, columns):
        summed = None
        for tap in range(window.shape[0]):
            term = window[tap, :, columns].astype(F32) * taps[tap : tap + 1, :]
            summed = term if summed is None else summed + term
        return summed

    every = pl.ds(0, width)
    taps_x = conv_x[...].astype(F32)
    taps_b = conv_b[:, group_cols].astype(F32)
    taps_c = conv_c[:, group_cols].astype(F32)
    last = taps_x.shape[0] - 1
    past_x = window_sum(window_x, taps_x, every)
    past_b = window_sum(window_b, taps_b, group_cols)
    past_c = window_sum(window_c, taps_c, group_cols)
    head_row = lax.broadcasted_iota(jnp.int32, (HEADS, width), 0)
    head_col = lax.broadcasted_iota(jnp.int32, (HEADS, width), 1) // HEAD_DIM + first_head
    spread = jnp.where(head_row == head_col, 1.0, 0.0)
    same_row = lax.broadcasted_iota(jnp.int32, (width, width), 0) // HEAD_DIM
    same_col = lax.broadcasted_iota(jnp.int32, (width, width), 1) // HEAD_DIM
    same_head = jnp.where(same_row == same_col, 1.0, 0.0).astype(BF)
    skip = dot32(jnp.broadcast_to(skip_gain[...], (8, HEADS)), spread, HIGH)[0:1, :]

    for step in range(1, n_tp):
        token_arrival(step).wait_recv()
    squares = jnp.zeros((seqs, 1), F32)
    for part in range(n_tp):
        piece = gathered[part].astype(F32)
        squares = squares + jnp.sum(piece * piece, axis=1, keepdims=True)
    scale = lax.rsqrt(squares / features + norm_epsilon)
    for part in range(n_tp):
        columns = slice(part * width, (part + 1) * width)
        piece = gathered[part].astype(F32)
        normed[:, columns] = (piece * scale * mix_gain[:, columns]).astype(BF)

    load_query.wait()
    query = silu(past_c + dot32(normed[...], w_query_c[...]) * taps_c[last : last + 1, :])
    queries[...] = query
    load_key.wait()
    key = silu(past_b + dot32(normed[...], w_key_b[...]) * taps_b[last : last + 1, :])
    key_query = jnp.sum(key * query, axis=1, keepdims=True)
    load_step.wait()
    raw_step = lax.dot_general(
        normed[...], w_step[...], (((1,), (1,)), ((), ())), preferred_element_type=F32
    )
    raw_step = raw_step + step_bias[...]
    step_size = jnp.maximum(raw_step, 0.0) + jnp.log1p(jnp.exp(-jnp.abs(raw_step)))
    decay = jnp.exp(-step_size * jnp.exp(decay_log[...]))
    step_wide = dot32(step_size, spread, HIGH)
    decay_wide = dot32(decay, spread, HIGH)
    load_value.wait()
    for tile in range(width // TILE):
        columns = slice(tile * TILE, (tile + 1) * TILE)
        values[:, columns] = silu(
            past_x[:, columns]
            + dot32(normed[...], w_value_x[:, columns]) * taps_x[last : last + 1, columns]
        )
    load_gate.wait()
    for tile in range(width // TILE):
        columns = slice(tile * TILE, (tile + 1) * TILE)
        gate_z[:, columns] = silu(dot32(normed[...], w_gate_z[:, columns]))

    def read_block(block, carry):
        load_state(block).wait()
        rows = pl.ds(pl.multiple_of(block * 8, 8), 8)
        asked = queries[rows, :].astype(BF)
        row_of = lax.broadcasted_iota(jnp.int32, (8, width), 0)
        total_read = jnp.zeros((8, width), F32)
        for row in range(8):
            held = state[block * 8 + row].astype(BF)
            found = lax.dot_general(
                asked, held, (((1,), (1,)), ((), ())), preferred_element_type=F32
            )
            total_read = jnp.where(row_of == row, found, total_read)
        state_read[rows, :] = total_read
        return carry

    lax.fori_loop(0, seqs // 8, read_block, 0)
    gated = decay_wide * state_read[...] + values[...] * (step_wide * key_query + skip)
    gated = gated * gate_z[...]
    squared = gated * gated
    squared_high = squared.astype(BF)
    squared_low = (squared - squared_high.astype(F32)).astype(BF)
    head_sum = dot32(squared_high, same_head) + dot32(squared_low, same_head)
    mixed = (gated * lax.rsqrt(head_sum / HEAD_DIM + norm_epsilon) * head_gain[...]).astype(BF)

    load_out.wait()

    def mix_copy(step):
        return pltpu.make_async_remote_copy(
            src_ref=mix_send.at[step],
            dst_ref=mix_recv.at[me_t],
            send_sem=mix_send_sem.at[step],
            recv_sem=mix_recv_sem.at[me_t],
            device_id=(me_e, lax.rem(me_t + step, n_tp)),
            device_id_type=MESH,
        )

    def mix_arrival(step):
        source = lax.rem(me_t + step, n_tp)
        return pltpu.make_async_remote_copy(
            src_ref=mix_send.at[step],
            dst_ref=mix_recv.at[source],
            send_sem=mix_send_sem.at[step],
            recv_sem=mix_recv_sem.at[source],
            device_id=(me_e, source),
            device_id_type=MESH,
        )

    for step in range(1, n_tp + 1):
        peer = lax.rem(me_t + step, n_tp)
        share = dot32(mixed, w_out[:, pl.ds(pl.multiple_of(peer * width, width), width)])
        if step < n_tp:
            mix_send[step] = share.astype(BF)
            mix_copy(step).start()
        else:
            mix_sum = share
    for step in range(1, n_tp):
        mix_arrival(step).wait_recv()
        mix_sum = mix_sum + mix_recv[lax.rem(me_t + step, n_tp)].astype(F32)
    residual = (tokens[...].astype(F32) + mix_sum).astype(BF)

    def row_copy(send, recv, send_sem, recv_sem, to_e, to_t, from_e, from_t):
        return pltpu.make_async_remote_copy(
            src_ref=send.at[to_e, to_t],
            dst_ref=recv.at[from_e, from_t],
            send_sem=send_sem.at[to_e, to_t],
            recv_sem=recv_sem.at[from_e, from_t],
            device_id=(to_e, to_t),
            device_id_type=MESH,
        )

    def spread_out(act, step_t):
        peer_t = lax.rem(me_t + step_t, n_tp)

        def one(step_e, carry):
            act(lax.rem(me_e + step_e, n_ep), peer_t)
            return carry

        lax.fori_loop(1 if step_t == 0 else 0, n_ep, one, 0)

    def start_row(to_e, to_t):
        row_copy(row_send, row_recv, row_send_sem, row_recv_sem, to_e, to_t, me_e, me_t).start()

    def await_row(from_e, from_t):
        row_copy(
            row_send, row_recv, row_send_sem, row_recv_sem, from_e, from_t, from_e, from_t
        ).wait_recv()

    def sent_row(to_e, to_t):
        row_copy(
            row_send, row_recv, row_send_sem, row_recv_sem, to_e, to_t, me_e, me_t
        ).wait_send()

    def start_back(to_e, to_t):
        row_copy(
            back_send, back_recv, back_send_sem, back_recv_sem, to_e, to_t, me_e, me_t
        ).start()

    def await_back(from_e, from_t):
        row_copy(
            back_send, back_recv, back_send_sem, back_recv_sem, from_e, from_t, from_e, from_t
        ).wait_recv()

    def sent_back(to_e, to_t):
        row_copy(
            back_send, back_recv, back_send_sem, back_recv_sem, to_e, to_t, me_e, me_t
        ).wait_send()

    outgoing = dot32(placed, residual)
    row_send[...] = outgoing.reshape(n_ep, n_tp, SLOT_ROWS, width).astype(BF)
    for step_t in range(n_tp):
        spread_out(start_row, step_t)
    row_recv[me_e, me_t] = row_send[me_e, me_t]
    for step_t in range(n_tp):
        spread_out(await_row, step_t)

    n_rows = n_ep * SLOT_ROWS
    squares = jnp.zeros((n_rows, 1), F32)
    for part in range(n_tp):
        piece = row_recv[:, part].astype(F32).reshape(n_rows, width)
        squares = squares + jnp.sum(piece * piece, axis=1, keepdims=True)
    scale = lax.rsqrt(squares / features + norm_epsilon)
    for part in range(n_tp):
        columns = slice(part * width, (part + 1) * width)
        piece = row_recv[:, part].astype(F32).reshape(n_rows, width)
        rows_in[:, columns] = (piece * scale * ffn_gain[:, columns]).astype(BF)
    load_exp_gate.wait()
    load_exp_up.wait()

    def expert_tile(tile, carry):
        columns = pl.ds(pl.multiple_of(tile * TILE, TILE), TILE)
        gate_part = dot32(rows_in[...], exp_gate[:, columns])
        up_part = dot32(rows_in[...], exp_up[:, columns])
        hidden[:, columns] = (silu(gate_part) * up_part).astype(BF)
        return carry

    lax.fori_loop(0, exp_gate.shape[1] // TILE, expert_tile, 0)
    load_exp_down.wait()
    for step_t in range(1, n_tp + 1):
        peer_t = lax.rem(me_t + step_t, n_tp)
        columns = pl.ds(pl.multiple_of(peer_t * width, width), width)
        result = dot32(hidden[...], exp_down[:, columns])
        back_send[:, peer_t] = result.reshape(n_ep, SLOT_ROWS, width).astype(BF)
        spread_out(start_back, step_t % n_tp)
    back_recv[me_e, me_t] = back_send[me_e, me_t]
    for step_t in range(n_tp):
        spread_out(await_back, step_t)
    returned = back_recv[...].astype(F32).reshape(n_slots, width).astype(BF)
    moe_sum = dot32(combine_high, returned) + dot32(combine_low, returned)
    out[...] = (residual.astype(F32) + moe_sum).astype(BF)

    for step in range(1, n_tp):
        token_copy(step).wait_send()
        mix_copy(step).wait_send()
    for step_t in range(n_tp):
        spread_out(sent_row, step_t)
        spread_out(sent_back, step_t)


def local(
    tokens,
    mix_gain,
    w_gate_z,
    w_value_x,
    w_key_b,
    w_query_c,
    w_step,
    step_bias,
    decay_log,
    skip_gain,
    conv_x_weight,
    conv_b_weight,
    conv_c_weight,
    window_x,
    window_b,
    window_c,
    ssm_state,
    head_gain,
    w_out,
    ffn_gain,
    route_ids,
    route_weights,
    expert_gate,
    expert_up,
    expert_down,
):
    n_ep, n_tp = lax.axis_size("ep"), lax.axis_size("tp")
    seqs, width = tokens.shape
    features = width * n_tp
    units = expert_gate.shape[2]
    capacity = -(-3 * seqs * route_ids.shape[1] // (2 * EXP_IN * n_ep))
    if n_tp != EXP_IN or width % TILE or units % TILE or seqs % 16 or capacity > SLOT_ROWS:
        return local_plain(
            tokens, mix_gain, w_gate_z, w_value_x, w_key_b, w_query_c, w_step, step_bias,
            decay_log, skip_gain, conv_x_weight, conv_b_weight, conv_c_weight, window_x,
            window_b, window_c, ssm_state, head_gain, w_out, ffn_gain, route_ids,
            route_weights, expert_gate, expert_up, expert_down,
        )
    state_rows = ssm_state.reshape(seqs, width, STATE)
    small = [
        tokens,
        mix_gain[None],
        step_bias[None],
        decay_log[None],
        skip_gain[None],
        conv_x_weight,
        conv_b_weight,
        conv_c_weight,
        window_x.transpose(1, 0, 2),
        window_b.transpose(1, 0, 2),
        window_c.transpose(1, 0, 2),
        head_gain[None],
        ffn_gain[None],
        route_ids.T,
        route_weights.T,
    ]
    large = [
        w_gate_z, w_value_x, w_key_b, w_query_c, w_step.T, state_rows, w_out,
        expert_gate[0], expert_up[0], expert_down[0],
    ]
    exchange = (n_ep, n_tp, SLOT_ROWS, width)
    vmem = pltpu.VMEM
    dma = pltpu.SemaphoreType.DMA
    return pl.pallas_call(
        functools.partial(layer_entry, n_ep, n_tp, len(small)),
        out_shape=jax.ShapeDtypeStruct((seqs, width), BF),
        in_specs=[pl.BlockSpec(memory_space=pl.ANY)] * (len(small) + len(large)),
        out_specs=pl.BlockSpec(memory_space=pltpu.VMEM),
        scratch_shapes=[
            vmem(w_gate_z.shape, BF),
            vmem(w_value_x.shape, BF),
            vmem((features, STATE), BF),
            vmem((features, STATE), BF),
            vmem(w_step.shape[::-1], BF),
            vmem(state_rows.shape, F32),
            vmem(w_out.shape, BF),
            vmem(expert_gate.shape[1:], BF),
            vmem(expert_up.shape[1:], BF),
            vmem(expert_down.shape[1:], BF),
            vmem((n_tp, seqs, width), BF),
            vmem((seqs, features), BF),
            vmem((seqs, width), F32),
            vmem((seqs, width), F32),
            vmem((seqs, STATE), F32),
            vmem((seqs, width), F32),
            vmem((n_tp, seqs, width), BF),
            vmem((n_tp, seqs, width), BF),
            vmem(exchange, BF),
            vmem(exchange, BF),
            vmem((n_ep * SLOT_ROWS, features), BF),
            vmem((n_ep * SLOT_ROWS, units), BF),
            vmem(exchange, BF),
            vmem(exchange, BF),
            dma((9,)),
            dma((seqs // 8,)),
            dma((n_tp,)),
            dma((n_tp,)),
            dma((n_tp,)),
            dma((n_tp,)),
            dma((n_ep, n_tp)),
            dma((n_ep, n_tp)),
            dma((n_ep, n_tp)),
            dma((n_ep, n_tp)),
            *[vmem(each.shape, each.dtype) for each in small],
            dma((len(small),)),
        ],
        compiler_params=pltpu.CompilerParams(
            collective_id=0, has_side_effects=True, vmem_limit_bytes=60 * 1024 * 1024
        ),
        name="layer",
    )(*small, *large)


def solution(mesh):
    in_specs = (
        P("ep", "tp"),
        P(),
        P(None, "tp"),
        P(None, "tp"),
        P(),
        P(),
        P(),
        P(),
        P(),
        P(),
        P(None, "tp"),
        P(),
        P(),
        P("ep", None, "tp"),
        P("ep", None, None),
        P("ep", None, None),
        P("ep", "tp", None, None),
        P("tp"),
        P("tp", None),
        P(),
        P("ep", None),
        P("ep", None),
        P("ep", None, "tp"),
        P("ep", None, "tp"),
        P("ep", "tp", None),
    )
    out_specs = P("ep", "tp")
    return jax.shard_map(local, mesh=mesh, in_specs=in_specs, out_specs=out_specs, check_vma=False)
```

profile of v0, /device:TPU:0, one launch (start us, length us, event | category | flops | bytes accessed | tf_op | source)
XLA Modules:
  0.0 43.0 jit_solution(13977133806451353207)
XLA Ops:
  0.0 41.5 %layer.1 = bf16[48,512]{1,0:T(8,128)(2,1)} custom-call(bf16[48,512]{1,0:T(8,128)(2,1)} %refs_0_.1, f32[1,2048]{1,0:T(1,128)} %bitcast.24, f32[1,32]{1,0:T(1,128)} %bitcast.29, f32[1,32]{1,0:T(1,128)} %bitcast.30, f32[1,32]{1,0:T(1,128)} %bitcast.31, bf16[4,512]{1,0:T(4,128)(2,1)} %refs_5_.1, bf16[4,256]{1,0:T(4,128)(2,1)} %refs_6_.1, ...), custom_call_target="tpu_custom_call" | custom-call | tf_op jit(solution)/shard_map/layer/pallas_call | solution.py:640
  41.6 1.4 %copy.27 = bf16[48,512]{1,0:T(8,128)(2,1)} copy(bf16[48,512]{1,0:T(8,128)(2,1)} %layer.1) | data formatting | bytes 98304
where the time goes:
time: 43.2 us; the launch traced here: 43 us
  Pallas kernels  41.5 us (96%)
  local copies, waits for them, and re-layouts  1.42 us (3%)
    pallas_call x1, Pallas kernels, local(): pl.pallas_call(functools.partial(layer_entry, n_ep, n_tp, len(small)), ou...  41.5 us
    unnamed x1, local copies, waits for them, and re-layouts  1.42 us

commit v1 on v0

v1 whole, which is shorter than its diff:
```python
import functools

import jax
import jax.numpy as jnp
from jax import lax
from jax.experimental import pallas as pl
from jax.experimental.pallas import tpu as pltpu
from jax.sharding import PartitionSpec as P

HEADS = 32
HEAD_DIM = 64
STATE = 128
GROUPS = 2
EXP_IN = 4


norm_epsilon = 1e-06


def row_norm(arr_values, norm_gain):
    widened = arr_values.astype(jnp.float32)
    return (
        widened
        * lax.rsqrt(jnp.mean(widened * widened, axis=-1, keepdims=True) + norm_epsilon)
        * norm_gain
    )


def short_conv(window, fresh_row, weight):
    conv_taps = weight.astype(jnp.float32)
    summed = (
        jnp.sum(window.astype(jnp.float32) * conv_taps[:-1][None], axis=1)
        + fresh_row * conv_taps[-1]
    )
    return jax.nn.silu(summed)


def product(left, right):
    return jnp.dot(left, right, preferred_element_type=jnp.float32)


def local_plain(
    tokens,
    mix_gain,
    w_gate_z,
    w_value_x,
    w_key_b,
    w_query_c,
    w_step,
    step_bias,
    decay_log,
    skip_gain,
    conv_x_weight,
    conv_b_weight,
    conv_c_weight,
    window_x,
    window_b,
    window_c,
    ssm_state,
    head_gain,
    w_out,
    ffn_gain,
    route_ids,
    route_weights,
    expert_gate,
    expert_up,
    expert_down,
):
    tp_index = lax.axis_index("tp")
    tp_count = lax.axis_size("tp")
    ep_count = lax.axis_size("ep")
    seq_count = tokens.shape[0]
    gathered = lax.all_gather(tokens, "tp", axis=1, tiled=True)
    normed = row_norm(gathered, mix_gain).astype(jnp.bfloat16)
    local_width = w_gate_z.shape[1]
    head_count = local_width // HEAD_DIM
    first_head = tp_index * head_count
    group_start = first_head // (HEADS // GROUPS) * STATE
    gate_z = product(normed, w_gate_z)
    values = short_conv(window_x, product(normed, w_value_x), conv_x_weight)
    key_b = short_conv(
        lax.dynamic_slice_in_dim(window_b, group_start, STATE, 2),
        product(normed, lax.dynamic_slice_in_dim(w_key_b, group_start, STATE, 1)),
        lax.dynamic_slice_in_dim(conv_b_weight, group_start, STATE, 1),
    )
    query_c = short_conv(
        lax.dynamic_slice_in_dim(window_c, group_start, STATE, 2),
        product(normed, lax.dynamic_slice_in_dim(w_query_c, group_start, STATE, 1)),
        lax.dynamic_slice_in_dim(conv_c_weight, group_start, STATE, 1),
    )
    step_all = product(normed, w_step) + step_bias
    step_size = jax.nn.softplus(lax.dynamic_slice_in_dim(step_all, first_head, head_count, 1))
    rate_heads = jnp.exp(lax.dynamic_slice_in_dim(decay_log, first_head, head_count, 0))
    skip_heads = lax.dynamic_slice_in_dim(skip_gain, first_head, head_count, 0)
    decay_heads = jnp.exp(-step_size * rate_heads)
    value_heads = values.reshape(seq_count, head_count, HEAD_DIM)
    new_state = (
        decay_heads[:, :, None, None] * ssm_state
        + (step_size[:, :, None] * value_heads)[..., None] * key_b[:, None, None, :]
    )
    read_out = jnp.einsum("shpn,sn->shp", new_state, query_c, precision=lax.Precision.HIGHEST)
    read_out = read_out + skip_heads[None, :, None] * value_heads
    gated = read_out * jax.nn.silu(gate_z.reshape(seq_count, head_count, HEAD_DIM))
    gated = gated * lax.rsqrt(jnp.mean(gated * gated, axis=-1, keepdims=True) + norm_epsilon)
    mixed_heads = (
        (gated * head_gain.reshape(head_count, HEAD_DIM))
        .reshape(seq_count, local_width)
        .astype(jnp.bfloat16)
    )
    partial_value = product(mixed_heads, w_out)
    share_mix = lax.psum_scatter(partial_value, "tp", scatter_dimension=1, tiled=True)
    residual_own = (tokens.astype(jnp.float32) + share_mix).astype(jnp.bfloat16)
    residual_full = lax.all_gather(residual_own, "tp", axis=1, tiled=True)
    ffn_in = row_norm(residual_full, ffn_gain).astype(jnp.bfloat16)
    top_count = route_ids.shape[1]
    expert_count = EXP_IN * ep_count
    capacity = max(2, (3 * seq_count * top_count + 2 * expert_count - 1) // (2 * expert_count))
    sub_index = tp_index // (tp_count // EXP_IN)
    target_set = route_ids // EXP_IN
    hit_mask = route_ids % EXP_IN == sub_index
    set_grid = jnp.arange(ep_count, dtype=jnp.int32)
    set_onehot = (hit_mask[:, :, None] & (target_set[:, :, None] == set_grid)).astype(jnp.int32)
    set_onehot = set_onehot.reshape(seq_count * top_count, ep_count)
    earlier = jnp.cumsum(set_onehot, axis=0) - set_onehot
    slot_rank = jnp.sum(earlier * set_onehot, axis=1).reshape(seq_count, top_count)
    slot_index = jnp.where(hit_mask, target_set * capacity + slot_rank, -1)
    slot_grid = jnp.arange(ep_count * capacity, dtype=jnp.int32)
    slot_match = slot_index[:, :, None] == slot_grid
    placed = jnp.any(slot_match, axis=1).astype(jnp.bfloat16)
    outgoing = jnp.einsum("sj,sd->jd", placed, ffn_in, preferred_element_type=jnp.float32)
    outgoing = outgoing.astype(jnp.bfloat16).reshape(ep_count, capacity, ffn_in.shape[1])
    route_share = route_weights / jnp.sum(route_weights, axis=1, keepdims=True)
    combine_weight = jnp.sum(jnp.where(slot_match, route_share[:, :, None], 0.0), axis=1)
    arrived = lax.all_to_all(outgoing, "ep", split_axis=0, concat_axis=0, tiled=True)
    source_count, slot_count, row_width = arrived.shape
    flat_rows = arrived.reshape(source_count * slot_count, row_width)
    gate_part = product(flat_rows, expert_gate[0])
    up_part = product(flat_rows, expert_up[0])
    hidden = (jax.nn.silu(gate_part) * up_part).astype(jnp.bfloat16)
    expert_out = product(hidden, expert_down[0]).reshape(source_count, slot_count, row_width)
    returned = lax.all_to_all(
        expert_out.astype(jnp.bfloat16), "ep", split_axis=0, concat_axis=0, tiled=True
    ).astype(expert_out.dtype)
    moe_part = jnp.dot(
        combine_weight,
        returned.reshape(ep_count * capacity, -1),
        precision=lax.Precision.HIGHEST,
        preferred_element_type=jnp.float32,
    )
    moe_share = lax.psum_scatter(
        moe_part.astype(jnp.bfloat16), "tp", scatter_dimension=1, tiled=True
    ).astype(jnp.float32)
    return (residual_own.astype(jnp.float32) + moe_share).astype(jnp.bfloat16)


MESH = pl.DeviceIdType.MESH
HIGH = lax.Precision.HIGHEST
BF = jnp.bfloat16
F32 = jnp.float32
LANES = 128
TILE = 256


def silu(v):
    return v / (1.0 + jnp.exp(-v))


def dot32(left, right, precision=None):
    return jnp.dot(left, right, preferred_element_type=F32, precision=precision)


def dot32_t(left, right):
    return lax.dot_general(left, right, (((1,), (1,)), ((), ())), preferred_element_type=F32)


def halves(v):
    high = v.astype(BF)
    return high, (v - high.astype(F32)).astype(BF)


def split_index(index, *counts):
    digits = []
    for place in range(len(counts) - 1):
        below = 1
        for count in counts[place + 1 :]:
            below = below * count
        digit = jnp.zeros_like(index)
        for step in range(1, counts[place]):
            digit = digit + jnp.where(index >= step * below, 1, 0)
        index = index - digit * below
        digits.append(digit)
    return (*digits, index)


_open = []


def mark(name):
    if _open:
        _open.pop().__exit__(None, None, None)
    if name:
        scope = jax.named_scope(name)
        scope.__enter__()
        _open.append(scope)


def layer_entry(n_ep, n_tp, slots, n_small, *refs):
    held, small_sem = refs[-1 - n_small : -1], refs[-1]
    fetches = [
        pltpu.make_async_copy(refs[at], held[at], small_sem.at[at]) for at in range(n_small)
    ]
    layer_kernel(n_ep, n_tp, slots, fetches, *held, *refs[n_small : -1 - n_small])


def layer_kernel(
    n_ep,
    n_tp,
    slots,
    fetches,
    tokens,
    mix_gain,
    step_bias,
    decay_log,
    skip_gain,
    conv_x,
    conv_b,
    conv_c,
    window_x,
    window_b,
    window_c,
    head_gain,
    ffn_gain,
    ids_t,
    scores_t,
    hbm_gate_z,
    hbm_value_x,
    hbm_key_b,
    hbm_query_c,
    hbm_step,
    hbm_state,
    hbm_out,
    hbm_exp_gate,
    hbm_exp_up,
    hbm_exp_down,
    out,
    w_gate_z,
    w_value_x,
    w_key_b,
    w_query_c,
    w_step,
    state,
    w_out,
    exp_gate,
    exp_up,
    exp_down,
    gathered,
    normed,
    queries,
    state_read,
    mix_send,
    mix_recv,
    row_send,
    row_recv,
    place,
    comb_high,
    comb_low,
    pick,
    unpick,
    sum_egate,
    sum_eup,
    hidden,
    back_send,
    back_recv,
    load_sem,
    state_sem,
    tok_send_sem,
    tok_recv_sem,
    mix_send_sem,
    mix_recv_sem,
    row_send_sem,
    row_recv_sem,
    back_send_sem,
    back_recv_sem,
):
    me_e = lax.axis_index("ep")
    me_t = lax.axis_index("tp")
    seqs, width = tokens.shape
    features = width * n_tp
    tiles = width // LANES
    lines = tiles * slots
    n_lines = n_ep * lines
    n_rows = n_ep * slots
    heads_here = width // HEAD_DIM
    first_head = me_t * heads_here
    group_start = pl.multiple_of(first_head // (HEADS // GROUPS) * STATE, STATE)
    group_cols = pl.ds(group_start, STATE)
    state_blocks = state_sem.shape[0]
    state_rows = seqs // state_blocks

    def peer(step):
        row, column = me_t // 2, lax.rem(me_t, 2)
        return lax.rem(row + step // 2, 2) * 2 + lax.rem(column + step % 2, 2)

    def other_e(step):
        return lax.rem(me_e + step, n_ep)

    far_first = sorted(range(n_ep), key=lambda step: -min(step, n_ep - step))
    steps = tuple(reversed(range(n_tp)))

    def load(source, target, index):
        return pltpu.make_async_copy(source, target, load_sem.at[index])

    load_key = load(hbm_key_b.at[:, group_cols], w_key_b, 0)
    load_query = load(hbm_query_c.at[:, group_cols], w_query_c, 1)
    load_step = load(hbm_step, w_step, 2)
    load_value = load(hbm_value_x, w_value_x, 3)
    load_gate = load(hbm_gate_z, w_gate_z, 4)
    load_out = load(hbm_out, w_out, 5)
    load_exp_gate = load(hbm_exp_gate, exp_gate, 6)
    load_exp_up = load(hbm_exp_up, exp_up, 7)
    load_exp_down = load(hbm_exp_down, exp_down, 8)

    def load_state(block):
        rows = pl.ds(block * state_rows, state_rows)
        return pltpu.make_async_copy(hbm_state.at[rows], state.at[rows], state_sem.at[block])

    mark("greet")
    for each in fetches:
        each.start()
    barrier = pltpu.get_barrier_semaphore()
    for step in range(1, n_tp):
        pl.semaphore_signal(
            barrier, inc=1, device_id=(me_e, peer(step)), device_id_type=MESH
        )
    for step in far_first:
        if step:
            pl.semaphore_signal(
                barrier, inc=1, device_id=(other_e(step), me_t), device_id_type=MESH
            )
    mark("loads")
    for each in (load_query, load_key, load_step, load_value, load_gate):
        each.start()
    for block in range(state_blocks):
        load_state(block).start(priority=1)
    mark("smallwait")
    for each in fetches:
        each.wait()
    mark("barrier")
    pl.semaphore_wait(barrier, n_tp + n_ep - 2)
    mark("toksend")

    def token_copy(step):
        return pltpu.make_async_remote_copy(
            src_ref=tokens,
            dst_ref=gathered.at[step - 1],
            send_sem=tok_send_sem,
            recv_sem=tok_recv_sem.at[step - 1],
            device_id=(me_e, peer(step)),
            device_id_type=MESH,
        )

    for step in reversed(range(1, n_tp)):
        token_copy(step).start()

    def part_rows(step):
        return pl.ds(pl.multiple_of(peer(step) * width, width), width)

    def squares_of(piece):
        wide = piece.astype(F32)
        return jnp.sum(wide * wide, axis=1, keepdims=True)

    mark("routes")
    n_exp = n_ep * EXP_IN
    row_at = lax.broadcasted_iota(jnp.int32, (seqs, seqs), 0)
    col_at = lax.broadcasted_iota(jnp.int32, (seqs, seqs), 1)

    def stood_up(row):
        return jnp.sum(jnp.where(row_at == col_at, row, 0.0), axis=1, keepdims=True)

    id0 = stood_up(ids_t[0:1, :].astype(F32)).astype(jnp.int32)
    id1 = stood_up(ids_t[1:2, :].astype(F32)).astype(jnp.int32)
    lane_exp = lax.broadcasted_iota(jnp.int32, (seqs, n_exp), 1)
    hit0 = jnp.where(id0 == lane_exp, 1.0, 0.0)
    hit1 = jnp.where(id1 == lane_exp, 1.0, 0.0)
    lower = jnp.where(row_at > col_at, 1.0, 0.0).astype(BF)
    upper = jnp.where(row_at < col_at, 1.0, 0.0).astype(BF)
    before = dot32(lower, (hit0 + hit1).astype(BF))
    slot0 = id0 * slots + jnp.sum(before * hit0, axis=1, keepdims=True).astype(jnp.int32)
    slot1 = id1 * slots + jnp.sum(before * hit1, axis=1, keepdims=True).astype(jnp.int32)
    score0, score1 = stood_up(scores_t[0:1, :]), stood_up(scores_t[1:2, :])
    total = score0 + score1

    def stacked(column):
        return jnp.concatenate([column] * tiles, axis=0)

    slot0, slot1 = stacked(slot0), stacked(slot1)
    share0, share1 = stacked(score0 / total), stacked(score1 / total)

    idt0, idt1 = ids_t[0:1, :], ids_t[1:2, :]
    sub_exp = lax.broadcasted_iota(jnp.int32, (n_exp, seqs), 0)
    hitt0 = jnp.where(idt0 == sub_exp, 1.0, 0.0)
    hitt1 = jnp.where(idt1 == sub_exp, 1.0, 0.0)
    before_t = dot32((hitt0 + hitt1).astype(BF), upper)
    rank0 = jnp.sum(before_t * hitt0, axis=0, keepdims=True)
    rank1 = jnp.sum(before_t * hitt1, axis=0, keepdims=True)
    rep_row = lax.broadcasted_iota(jnp.int32, (seqs, tiles * seqs), 0)
    rep_col = lax.broadcasted_iota(jnp.int32, (1, tiles * seqs), 1)
    tile_col, token_col = split_index(rep_col, tiles, seqs)
    repeat = jnp.where(rep_row == token_col, 1.0, 0.0).astype(BF)
    wide_ids = dot32(
        jnp.concatenate([idt0.astype(F32), idt1.astype(F32), rank0, rank1] * 2, axis=0).astype(BF),
        repeat,
    ).astype(jnp.int32)
    slott0 = wide_ids[0:1, :] * slots + wide_ids[2:3, :]
    slott1 = wide_ids[1:2, :] * slots + wide_ids[3:4, :]

    line_row = lax.broadcasted_iota(jnp.int32, (n_lines, 1), 0)
    e_row, c_row, k_row = split_index(line_row, n_ep, tiles, slots)
    line_col = lax.broadcasted_iota(jnp.int32, (1, n_lines), 1)
    e_col, c_col, k_col = split_index(line_col, n_ep, tiles, slots)
    tok_row = lax.broadcasted_iota(jnp.int32, (tiles * seqs, 1), 0)
    tile_row, _ = split_index(tok_row, tiles, seqs)
    pick[...] = jnp.where(
        line_row == c_col * n_rows + e_col * slots + k_col, 1.0, 0.0
    ).astype(BF)
    unpick[...] = jnp.where(
        line_col == c_row * n_rows + e_row * slots + k_row, 1.0, 0.0
    ).astype(BF)
    for step in range(n_tp):
        there_row = (e_row * n_tp + peer(step)) * slots + k_row
        there_col = (e_col * n_tp + peer(step)) * slots + k_col
        same = c_row == tile_col
        chosen = same & ((slott0 == there_row) | (slott1 == there_row))
        place[step] = jnp.where(chosen, 1.0, 0.0).astype(BF)
        same = tile_row == c_col
        weight = jnp.where(same & (slot0 == there_col), share0, 0.0) + jnp.where(
            same & (slot1 == there_col), share1, 0.0
        )
        comb_high[step], comb_low[step] = halves(weight)

    mark("pasts")

    def window_sum(window, taps, columns):
        summed = None
        for tap in range(window.shape[0]):
            term = window[tap, :, columns].astype(F32) * taps[tap : tap + 1, :]
            summed = term if summed is None else summed + term
        return summed

    every = pl.ds(0, width)
    taps_x = conv_x[...].astype(F32)
    taps_b = conv_b[:, group_cols].astype(F32)
    taps_c = conv_c[:, group_cols].astype(F32)
    last = taps_x.shape[0] - 1
    past_x = window_sum(window_x, taps_x, every)
    past_b = window_sum(window_b, taps_b, group_cols)
    past_c = window_sum(window_c, taps_c, group_cols)
    head_row = lax.broadcasted_iota(jnp.int32, (HEADS, width), 0)
    head_col = lax.broadcasted_iota(jnp.int32, (HEADS, width), 1) // HEAD_DIM + first_head
    spread = jnp.where(head_row == head_col, 1.0, 0.0).astype(BF)
    same_row = lax.rem(lax.broadcasted_iota(jnp.int32, (2 * LANES, LANES), 0), LANES) // HEAD_DIM
    same_col = lax.broadcasted_iota(jnp.int32, (2 * LANES, LANES), 1) // HEAD_DIM
    same_head = jnp.where(same_row == same_col, 1.0, 0.0).astype(BF)
    skip = dot32(jnp.broadcast_to(skip_gain[...], (8, HEADS)), spread.astype(F32), HIGH)[0:1, :]

    squares = squares_of(tokens[...])
    for step in range(1, n_tp):
        mark(f"tokwait{step}")
        token_copy(step).wait_recv()
        squares = squares + squares_of(gathered[step - 1])
    mark("norm")
    for each in (load_out, load_exp_gate, load_exp_up, load_exp_down):
        each.start(priority=1)
    scale = lax.rsqrt(squares / features + norm_epsilon)
    for step in range(n_tp):
        piece = gathered[step - 1] if step else tokens[...]
        columns = part_rows(step)
        normed[:, columns] = (piece.astype(F32) * scale * mix_gain[:, columns]).astype(BF)
    mark("projwait")
    for each in (load_query, load_key, load_step, load_value, load_gate):
        each.wait()
    mark("query")
    query = silu(past_c + dot32(normed[...], w_query_c[...]) * taps_c[last : last + 1, :])
    queries[...] = query
    key = silu(past_b + dot32(normed[...], w_key_b[...]) * taps_b[last : last + 1, :])
    key_query = jnp.sum(key * query, axis=1, keepdims=True)
    raw_step = dot32_t(normed[...], w_step[...]) + step_bias[...]
    step_size = jnp.maximum(raw_step, 0.0) + jnp.log1p(jnp.exp(-jnp.abs(raw_step)))
    decay = jnp.exp(-step_size * jnp.exp(decay_log[...]))
    spread_high, spread_low = halves(jnp.concatenate([step_size, decay], axis=0))
    wide = dot32(jnp.concatenate([spread_high, spread_low], axis=0), spread)
    step_wide = wide[0:seqs] + wide[2 * seqs : 3 * seqs]
    decay_wide = wide[seqs : 2 * seqs] + wide[3 * seqs : 4 * seqs]
    mark("value")
    values = silu(past_x + dot32(normed[...], w_value_x[...]) * taps_x[last : last + 1, :])
    direct = values * (step_wide * key_query + skip)
    gate_z = silu(dot32(normed[...], w_gate_z[...]))

    mark("state")

    def read_block(block, carry):
        rows = pl.ds(pl.multiple_of(block * 8, 8), 8)
        asked = queries[rows, :].astype(BF)
        row_of = lax.broadcasted_iota(jnp.int32, (8, width), 0)
        total_read = jnp.zeros((8, width), F32)
        for row in range(8):
            held = state[block * 8 + row].astype(BF)
            total_read = jnp.where(row_of == row, dot32_t(asked, held), total_read)
        state_read[rows, :] = total_read
        return carry

    for block in range(state_blocks):
        mark(f"statewait{block}")
        load_state(block).wait()
    mark("state")
    lax.fori_loop(0, seqs // 8, read_block, 0)

    mark("gated")
    gated = (decay_wide * state_read[...] + direct) * gate_z
    squared = gated * gated
    squared = jnp.concatenate(
        [squared[:, tile * LANES : (tile + 1) * LANES] for tile in range(tiles)], axis=0
    )
    head_sum = dot32(jnp.concatenate(halves(squared), axis=1), same_head)
    norm = lax.rsqrt(head_sum / HEAD_DIM + norm_epsilon)
    norm = jnp.concatenate(
        [norm[tile * seqs : (tile + 1) * seqs, :] for tile in range(tiles)], axis=1
    )
    mixed = (gated * norm * head_gain[...]).astype(BF)

    mark("outproj")
    load_out.wait()

    def mix_copy(step):
        return pltpu.make_async_remote_copy(
            src_ref=mix_send.at[step - 1],
            dst_ref=mix_recv.at[step - 1],
            send_sem=mix_send_sem,
            recv_sem=mix_recv_sem,
            device_id=(me_e, peer(step)),
            device_id_type=MESH,
        )

    def all_mixes():
        return pltpu.make_async_remote_copy(
            src_ref=mix_send,
            dst_ref=mix_recv,
            send_sem=mix_send_sem,
            recv_sem=mix_recv_sem,
            device_id=(me_e, peer(1)),
            device_id_type=MESH,
        )

    for step in steps:
        share = dot32(mixed, w_out[:, part_rows(step)])
        if step:
            mix_send[step - 1] = share.astype(BF)
            mix_copy(step).start()
        else:
            mix_sum = share
    mark("mixwait")
    all_mixes().wait_recv()
    mark("residual")
    for step in range(1, n_tp):
        mix_sum = mix_sum + mix_recv[step - 1].astype(F32)
    residual = (tokens[...].astype(F32) + mix_sum).astype(BF)

    def chunk(step):
        return pl.ds(step * n_ep, n_ep)

    def exchange(send, recv, send_sem, recv_sem, step, step_e):
        return pltpu.make_async_remote_copy(
            src_ref=send.at[step * n_ep + other_e(step_e)],
            dst_ref=recv.at[step * n_ep + me_e],
            send_sem=send_sem,
            recv_sem=recv_sem.at[step],
            device_id=(other_e(step_e), peer(step)),
            device_id_type=MESH,
        )

    def send_out(send, recv, send_sem, recv_sem, step):
        for step_e in far_first:
            if step or step_e:
                exchange(send, recv, send_sem, recv_sem, step, step_e).start()
        if step == 0:
            recv[me_e] = send[me_e]

    def await_chunk(send, recv, send_sem, recv_sem, step):
        blocks = chunk(step) if step else pl.ds(0, n_ep - 1)
        pltpu.make_async_remote_copy(
            src_ref=send.at[blocks],
            dst_ref=recv.at[blocks],
            send_sem=send_sem,
            recv_sem=recv_sem.at[step],
            device_id=(me_e, peer(1)),
            device_id_type=MESH,
        ).wait_recv()

    def await_sent(send, recv, send_sem, recv_sem):
        blocks = pl.ds(0, n_ep * n_tp - 1)
        pltpu.make_async_remote_copy(
            src_ref=send.at[blocks],
            dst_ref=recv.at[blocks],
            send_sem=send_sem,
            recv_sem=recv_sem.at[0],
            device_id=(me_e, peer(1)),
            device_id_type=MESH,
        ).wait_send()

    out_rows = (row_send, row_recv, row_send_sem, row_recv_sem)
    back_rows = (back_send, back_recv, back_send_sem, back_recv_sem)
    stack = jnp.concatenate(
        [residual[:, tile * LANES : (tile + 1) * LANES] for tile in range(tiles)], axis=0
    )
    for step in steps:
        mark(f"place{step}")
        outgoing = dot32(place[step], stack).astype(BF)
        row_send[chunk(step)] = outgoing.reshape(n_ep, lines, LANES)
        mark(f"rowsend{step}")
        send_out(*out_rows, step)

    mark("expwait")
    load_exp_gate.wait()
    load_exp_up.wait()
    load_exp_down.wait()
    pltpu.make_async_remote_copy(
        src_ref=gathered,
        dst_ref=gathered,
        send_sem=tok_send_sem,
        recv_sem=tok_recv_sem.at[0],
        device_id=(me_e, peer(1)),
        device_id_type=MESH,
    ).wait_send()
    all_mixes().wait_send()

    units = exp_gate.shape[1]
    squares = jnp.zeros((n_rows, 1), F32)
    for step in steps:
        mark(f"rowwait{step}")
        await_chunk(*out_rows, step)
        mark(f"gateup{step}")
        came = dot32(pick[...], row_recv[chunk(step)].reshape(n_lines, LANES))
        rows = part_rows(step)
        pieces = [came[tile * n_rows : (tile + 1) * n_rows, :] for tile in range(tiles)]
        for piece in pieces:
            squares = squares + jnp.sum(piece * piece, axis=1, keepdims=True)
        left = (jnp.concatenate(pieces, axis=1) * ffn_gain[:, rows]).astype(BF)
        scale = lax.rsqrt(squares / features + norm_epsilon)
        for at in range(units // TILE):
            columns = slice(at * TILE, (at + 1) * TILE)
            gate_part = dot32(left, exp_gate[rows, columns])
            up_part = dot32(left, exp_up[rows, columns])
            if step != steps[0]:
                gate_part = sum_egate[:, columns] + gate_part
                up_part = sum_eup[:, columns] + up_part
            if step != steps[-1]:
                sum_egate[:, columns] = gate_part
                sum_eup[:, columns] = up_part
            else:
                hidden[:, columns] = (silu(gate_part * scale) * (up_part * scale)).astype(BF)
    mark("down")

    def expert_part(step):
        result = dot32(hidden[...], exp_down[:, part_rows(step)]).astype(BF)
        return jnp.concatenate(
            [result[:, tile * LANES : (tile + 1) * LANES] for tile in range(tiles)], axis=0
        )

    part = expert_part(steps[0])
    for at, step in enumerate(steps):
        ready = part
        if at + 1 < n_tp:
            part = expert_part(steps[at + 1])
        back_send[chunk(step)] = dot32(unpick[...], ready).astype(BF).reshape(n_ep, lines, LANES)
        send_out(*back_rows, step)
    mark("rowdrain")
    await_sent(*out_rows)
    moe_sum = jnp.zeros((tiles * seqs, LANES), F32)
    for step in range(n_tp):
        mark(f"backwait{step}")
        await_chunk(*back_rows, step)
        mark(f"combine{step}")
        came = back_recv[chunk(step)].reshape(n_lines, LANES)
        moe_sum = moe_sum + dot32(comb_high[step], came) + dot32(comb_low[step], came)
    for tile in range(tiles):
        columns = slice(tile * LANES, (tile + 1) * LANES)
        part = moe_sum[tile * seqs : (tile + 1) * seqs, :]
        out[:, columns] = (residual[:, columns].astype(F32) + part).astype(BF)
    mark("drain")
    await_sent(*back_rows)
    mark(None)


def local(
    tokens,
    mix_gain,
    w_gate_z,
    w_value_x,
    w_key_b,
    w_query_c,
    w_step,
    step_bias,
    decay_log,
    skip_gain,
    conv_x_weight,
    conv_b_weight,
    conv_c_weight,
    window_x,
    window_b,
    window_c,
    ssm_state,
    head_gain,
    w_out,
    ffn_gain,
    route_ids,
    route_weights,
    expert_gate,
    expert_up,
    expert_down,
):
    n_ep, n_tp = lax.axis_size("ep"), lax.axis_size("tp")
    seqs, width = tokens.shape
    features = width * n_tp
    units = expert_gate.shape[2]
    slots = -(-3 * seqs * route_ids.shape[1] // (2 * EXP_IN * n_ep))
    while slots * (width // LANES) % 8:
        slots = slots + 1
    if (
        n_tp != EXP_IN
        or n_tp != 4
        or route_ids.shape[1] != 2
        or width % LANES
        or units % TILE
        or seqs % 16
        or n_ep * slots % 16
        or n_ep * EXP_IN > 256
    ):
        return local_plain(
            tokens, mix_gain, w_gate_z, w_value_x, w_key_b, w_query_c, w_step, step_bias,
            decay_log, skip_gain, conv_x_weight, conv_b_weight, conv_c_weight, window_x,
            window_b, window_c, ssm_state, head_gain, w_out, ffn_gain, route_ids,
            route_weights, expert_gate, expert_up, expert_down,
        )
    state_rows = ssm_state.reshape(seqs, width, STATE)
    small = [
        tokens,
        mix_gain[None],
        step_bias[None],
        decay_log[None],
        skip_gain[None],
        conv_x_weight,
        conv_b_weight,
        conv_c_weight,
        window_x.transpose(1, 0, 2),
        window_b.transpose(1, 0, 2),
        window_c.transpose(1, 0, 2),
        head_gain[None],
        ffn_gain[None],
        route_ids.T,
        route_weights.T,
    ]
    large = [
        w_gate_z, w_value_x, w_key_b, w_query_c, w_step.T, state_rows, w_out,
        expert_gate[0], expert_up[0], expert_down[0],
    ]
    operands = [pltpu.with_memory_space_constraint(each, pltpu.HBM) for each in small + large]
    tiles = width // LANES
    n_rows = n_ep * slots
    n_lines = n_rows * tiles
    exchange = (n_ep * n_tp, tiles * slots, LANES)
    vmem = pltpu.VMEM
    dma = pltpu.SemaphoreType.DMA
    return pl.pallas_call(
        functools.partial(layer_entry, n_ep, n_tp, slots, len(small)),
        out_shape=pltpu.VMEM((seqs, width), BF),
        in_specs=[pl.BlockSpec(memory_space=pl.ANY)] * len(operands),
        out_specs=pl.BlockSpec(memory_space=pltpu.VMEM),
        scratch_shapes=[
            vmem(w_gate_z.shape, BF),
            vmem(w_value_x.shape, BF),
            vmem((features, STATE), BF),
            vmem((features, STATE), BF),
            vmem(w_step.shape[::-1], BF),
            vmem(state_rows.shape, F32),
            vmem(w_out.shape, BF),
            vmem(expert_gate.shape[1:], BF),
            vmem(expert_up.shape[1:], BF),
            vmem(expert_down.shape[1:], BF),
            vmem((n_tp - 1, seqs, width), BF),
            vmem((seqs, features), BF),
            vmem((seqs, STATE), F32),
            vmem((seqs, width), F32),
            vmem((n_tp - 1, seqs, width), BF),
            vmem((n_tp - 1, seqs, width), BF),
            vmem(exchange, BF),
            vmem(exchange, BF),
            vmem((n_tp, n_lines, tiles * seqs), BF),
            vmem((n_tp, tiles * seqs, n_lines), BF),
            vmem((n_tp, tiles * seqs, n_lines), BF),
            vmem((n_lines, n_lines), BF),
            vmem((n_lines, n_lines), BF),
            vmem((n_rows, units), F32),
            vmem((n_rows, units), F32),
            vmem((n_rows, units), BF),
            vmem(exchange, BF),
            vmem(exchange, BF),
            dma((9,)),
            dma((2,)),
            dma,
            dma((n_tp - 1,)),
            dma,
            dma,
            dma,
            dma((n_tp,)),
            dma,
            dma((n_tp,)),
            *[vmem(each.shape, each.dtype) for each in small],
            dma((len(small),)),
        ],
        compiler_params=pltpu.CompilerParams(
            collective_id=0, has_side_effects=True, vmem_limit_bytes=60 * 1024 * 1024
        ),
        name="layer",
    )(*operands)


def solution(mesh):
    in_specs = (
        P("ep", "tp"),
        P(),
        P(None, "tp"),
        P(None, "tp"),
        P(),
        P(),
        P(),
        P(),
        P(),
        P(),
        P(None, "tp"),
        P(),
        P(),
        P("ep", None, "tp"),
        P("ep", None, None),
        P("ep", None, None),
        P("ep", "tp", None, None),
        P("tp"),
        P("tp", None),
        P(),
        P("ep", None),
        P("ep", None),
        P("ep", None, "tp"),
        P("ep", None, "tp"),
        P("ep", "tp", None),
    )
    out_specs = P("ep", "tp")
    return jax.shard_map(local, mesh=mesh, in_specs=in_specs, out_specs=out_specs, check_vma=False)
```

time: 43.2 us -> 33.7 us (0.78)
  Pallas kernels: 41.5 us -> 32.9 us
  local copies, waits for them, and re-layouts: 1.42 us -> 0.62 us
    pallas_call x1, Pallas kernels: 41.5 us -> 32.9 us  [local(): pl.pallas_call(functools.partial(layer_entry, n_ep, n_tp, slots, len(smal...]
    unnamed x1, local copies, waits for them, and re-layouts: 1.42 us -> 0.62 us
where the time goes in v1:
time: 33.7 us; the launch traced here: 33.6 us
  Pallas kernels  32.9 us (98%)
  local copies, waits for them, and re-layouts  0.62 us (2%)
    pallas_call x1, Pallas kernels, local(): pl.pallas_call(functools.partial(layer_entry, n_ep, n_tp, slots, len(smal...  32.9 us

profile of v1, /device:TPU:0, one launch (start us, length us, event | category | flops | bytes accessed | tf_op | source)
XLA Modules:
  0.0 33.6 jit_solution(10097280129181458448)
XLA Ops:
  0.0 32.9 %layer.1 = bf16[48,512]{1,0:T(8,128)(2,1)S(1)} custom-call(bf16[48,512]{1,0:T(8,128)(2,1)} %refs_0_.1, f32[1,2048]{1,0:T(1,128)} %bitcast.24, f32[1,32]{1,0:T(1,128)} %bitcast.29, f32[1,32]{1,0:T(1,128)} %bitcast.30, f32[1,32]{1,0:T(1,128)} %bitcast.31, bf16[4,512]{1,0:T(4,128)(2,1)} %refs_5_.1, bf16[4,256]{1,0:T(4,128)(2,1)} %refs_6_.1, ...), custom_call_target="tpu_custom_call" | custom-call | tf_op jit(solution)/shard_map/layer/pallas_call | solution.py:773
  33.0 0.6 %copy.27 = bf16[48,512]{1,0:T(8,128)(2,1)} copy(bf16[48,512]{1,0:T(8,128)(2,1)S(1)} %layer.1) | data formatting | bytes 98304

commit v2 on v1

--- a/solution.py
+++ b/solution.py
@@ -159,6 +159,7 @@
 F32 = jnp.float32
 LANES = 128
 TILE = 256
+ROW_SEND, ROW_USE = (0, 1, 2, 3), (0, 1, 2, 3)
 
 
 def silu(v):
@@ -281,15 +282,16 @@
     row_recv_sem,
     back_send_sem,
     back_recv_sem,
+    chain_sem,
 ):
     me_e = lax.axis_index("ep")
     me_t = lax.axis_index("tp")
     seqs, width = tokens.shape
     features = width * n_tp
     tiles = width // LANES
-    lines = tiles * slots
-    n_lines = n_ep * lines
-    n_rows = n_ep * slots
+    n_lines = n_ep * slots * tiles
+    n_rows = hidden.shape[0]
+    carried = (n_ep, slots, tiles, LANES)
     heads_here = width // HEAD_DIM
     first_head = me_t * heads_here
     group_start = pl.multiple_of(first_head // (HEADS // GROUPS) * STATE, STATE)
@@ -332,21 +334,58 @@
         pl.semaphore_signal(
             barrier, inc=1, device_id=(me_e, peer(step)), device_id_type=MESH
         )
-    for step in far_first:
-        if step:
-            pl.semaphore_signal(
-                barrier, inc=1, device_id=(other_e(step), me_t), device_id_type=MESH
-            )
+    partner = me_e // 2 * 2 + 1 - lax.rem(me_e, 2)
+    has_below = (me_e + n_ep - 2) // n_ep
+    has_above = (2 * n_ep - 3 - me_e) // n_ep
+
+    def signal_e(semaphore, to_e):
+        pl.semaphore_signal(semaphore, inc=1, device_id=(to_e, me_t), device_id_type=MESH)
+
+    signal_e(barrier, partner)
+
+    @pl.when(has_below == 1)
+    def _():
+        signal_e(barrier, me_e - 2)
+
+    @pl.when(has_above == 1)
+    def _():
+        signal_e(barrier, me_e + 2)
+
+    def chain_send(turn):
+        @pl.when(has_below == 1)
+        def _():
+            signal_e(chain_sem.at[turn, 0], me_e - 2)
+
+        @pl.when(has_above == 1)
+        def _():
+            signal_e(chain_sem.at[turn, 1], me_e + 2)
+
+    def chain_wait(turn):
+        @pl.when(has_above == 1)
+        def _():
+            pl.semaphore_wait(chain_sem.at[turn, 0], 1)
+
+        @pl.when(has_below == 1)
+        def _():
+            pl.semaphore_wait(chain_sem.at[turn, 1], 1)
+
+    turns = n_ep // 2 - 1
+
+    def turn_on(start, stop):
+        for turn in range(start, stop):
+            if turn < turns:
+                chain_wait(turn - 1)
+                chain_send(turn)
+
     mark("loads")
     for each in (load_query, load_key, load_step, load_value, load_gate):
         each.start()
     for block in range(state_blocks):
         load_state(block).start(priority=1)
     mark("smallwait")
-    for each in fetches:
-        each.wait()
+    fetches[0].wait()
     mark("barrier")
-    pl.semaphore_wait(barrier, n_tp + n_ep - 2)
+    pl.semaphore_wait(barrier, n_tp + has_below + has_above)
     mark("toksend")
 
     def token_copy(step):
@@ -361,6 +400,10 @@
 
     for step in reversed(range(1, n_tp)):
         token_copy(step).start()
+    chain_send(0)
+    mark("smallrest")
+    for each in fetches[1:]:
+        each.wait()
 
     def part_rows(step):
         return pl.ds(pl.multiple_of(peer(step) * width, width), width)
@@ -415,16 +458,18 @@
     slott1 = wide_ids[1:2, :] * slots + wide_ids[3:4, :]
 
     line_row = lax.broadcasted_iota(jnp.int32, (n_lines, 1), 0)
-    e_row, c_row, k_row = split_index(line_row, n_ep, tiles, slots)
+    e_row, k_row, c_row = split_index(line_row, n_ep, slots, tiles)
     line_col = lax.broadcasted_iota(jnp.int32, (1, n_lines), 1)
-    e_col, c_col, k_col = split_index(line_col, n_ep, tiles, slots)
+    e_col, k_col, c_col = split_index(line_col, n_ep, slots, tiles)
     tok_row = lax.broadcasted_iota(jnp.int32, (tiles * seqs, 1), 0)
     tile_row, _ = split_index(tok_row, tiles, seqs)
+    pick_row = lax.broadcasted_iota(jnp.int32, (tiles * n_rows, 1), 0)
     pick[...] = jnp.where(
-        line_row == c_col * n_rows + e_col * slots + k_col, 1.0, 0.0
+        pick_row == c_col * n_rows + e_col * slots + k_col, 1.0, 0.0
     ).astype(BF)
+    pick_col = lax.broadcasted_iota(jnp.int32, (1, tiles * n_rows), 1)
     unpick[...] = jnp.where(
-        line_col == c_row * n_rows + e_row * slots + k_row, 1.0, 0.0
+        pick_col == c_row * n_rows + e_row * slots + k_row, 1.0, 0.0
     ).astype(BF)
     for step in range(n_tp):
         there_row = (e_row * n_tp + peer(step)) * slots + k_row
@@ -476,12 +521,12 @@
         piece = gathered[step - 1] if step else tokens[...]
         columns = part_rows(step)
         normed[:, columns] = (piece.astype(F32) * scale * mix_gain[:, columns]).astype(BF)
+    turn_on(1, 2)
     mark("projwait")
     for each in (load_query, load_key, load_step, load_value, load_gate):
         each.wait()
     mark("query")
     query = silu(past_c + dot32(normed[...], w_query_c[...]) * taps_c[last : last + 1, :])
-    queries[...] = query
     key = silu(past_b + dot32(normed[...], w_key_b[...]) * taps_b[last : last + 1, :])
     key_query = jnp.sum(key * query, axis=1, keepdims=True)
     raw_step = dot32_t(normed[...], w_step[...]) + step_bias[...]
@@ -498,7 +543,11 @@
 
     mark("state")
 
+    queries[...] = query
+    turn_on(2, turns)
+
     def read_block(block, carry):
+        load_state(block).wait()
         rows = pl.ds(pl.multiple_of(block * 8, 8), 8)
         asked = queries[rows, :].astype(BF)
         row_of = lax.broadcasted_iota(jnp.int32, (8, width), 0)
@@ -509,12 +558,7 @@
         state_read[rows, :] = total_read
         return carry
 
-    for block in range(state_blocks):
-        mark(f"statewait{block}")
-        load_state(block).wait()
-    mark("state")
     lax.fori_loop(0, seqs // 8, read_block, 0)
-
     mark("gated")
     gated = (decay_wide * state_read[...] + direct) * gate_z
     squared = gated * gated
@@ -529,6 +573,7 @@
     mixed = (gated * norm * head_gain[...]).astype(BF)
 
     mark("outproj")
+    chain_wait(turns - 1)
     load_out.wait()
 
     def mix_copy(step):
@@ -612,10 +657,10 @@
     stack = jnp.concatenate(
         [residual[:, tile * LANES : (tile + 1) * LANES] for tile in range(tiles)], axis=0
     )
-    for step in steps:
+    for step in ROW_SEND:
         mark(f"place{step}")
         outgoing = dot32(place[step], stack).astype(BF)
-        row_send[chunk(step)] = outgoing.reshape(n_ep, lines, LANES)
+        row_send[chunk(step)] = outgoing.reshape(carried)
         mark(f"rowsend{step}")
         send_out(*out_rows, step)
 
@@ -635,7 +680,7 @@
 
     units = exp_gate.shape[1]
     squares = jnp.zeros((n_rows, 1), F32)
-    for step in steps:
+    for step in ROW_USE:
         mark(f"rowwait{step}")
         await_chunk(*out_rows, step)
         mark(f"gateup{step}")
@@ -650,10 +695,10 @@
             columns = slice(at * TILE, (at + 1) * TILE)
             gate_part = dot32(left, exp_gate[rows, columns])
             up_part = dot32(left, exp_up[rows, columns])
-            if step != steps[0]:
+            if step != ROW_USE[0]:
                 gate_part = sum_egate[:, columns] + gate_part
                 up_part = sum_eup[:, columns] + up_part
-            if step != steps[-1]:
+            if step != ROW_USE[-1]:
                 sum_egate[:, columns] = gate_part
                 sum_eup[:, columns] = up_part
             else:
@@ -661,22 +706,22 @@
     mark("down")
 
     def expert_part(step):
-        result = dot32(hidden[...], exp_down[:, part_rows(step)]).astype(BF)
+        result = dot32(hidden[...], exp_down[:, part_rows(step)])
         return jnp.concatenate(
             [result[:, tile * LANES : (tile + 1) * LANES] for tile in range(tiles)], axis=0
-        )
+        ).astype(BF)
 
     part = expert_part(steps[0])
     for at, step in enumerate(steps):
         ready = part
         if at + 1 < n_tp:
             part = expert_part(steps[at + 1])
-        back_send[chunk(step)] = dot32(unpick[...], ready).astype(BF).reshape(n_ep, lines, LANES)
+        back_send[chunk(step)] = dot32(unpick[...], ready).astype(BF).reshape(carried)
         send_out(*back_rows, step)
     mark("rowdrain")
     await_sent(*out_rows)
     moe_sum = jnp.zeros((tiles * seqs, LANES), F32)
-    for step in range(n_tp):
+    for step in steps:
         mark(f"backwait{step}")
         await_chunk(*back_rows, step)
         mark(f"combine{step}")
@@ -723,8 +768,6 @@
     features = width * n_tp
     units = expert_gate.shape[2]
     slots = -(-3 * seqs * route_ids.shape[1] // (2 * EXP_IN * n_ep))
-    while slots * (width // LANES) % 8:
-        slots = slots + 1
     if (
         n_tp != EXP_IN
         or n_tp != 4
@@ -732,7 +775,9 @@
         or width % LANES
         or units % TILE
         or seqs % 16
-        or n_ep * slots % 16
+        or n_ep * slots * (width // LANES) % 16
+        or n_ep % 2
+        or n_ep < 4
         or n_ep * EXP_IN > 256
     ):
         return local_plain(
@@ -765,9 +810,9 @@
     ]
     operands = [pltpu.with_memory_space_constraint(each, pltpu.HBM) for each in small + large]
     tiles = width // LANES
-    n_rows = n_ep * slots
-    n_lines = n_rows * tiles
-    exchange = (n_ep * n_tp, tiles * slots, LANES)
+    n_lines = n_ep * slots * tiles
+    n_rows = -(-n_ep * slots // 16) * 16
+    exchange = (n_ep * n_tp, slots, tiles, LANES)
     vmem = pltpu.VMEM
     dma = pltpu.SemaphoreType.DMA
     return pl.pallas_call(
@@ -797,15 +842,15 @@
             vmem((n_tp, n_lines, tiles * seqs), BF),
             vmem((n_tp, tiles * seqs, n_lines), BF),
             vmem((n_tp, tiles * seqs, n_lines), BF),
-            vmem((n_lines, n_lines), BF),
-            vmem((n_lines, n_lines), BF),
+            vmem((tiles * n_rows, n_lines), BF),
+            vmem((n_lines, tiles * n_rows), BF),
             vmem((n_rows, units), F32),
             vmem((n_rows, units), F32),
             vmem((n_rows, units), BF),
             vmem(exchange, BF),
             vmem(exchange, BF),
             dma((9,)),
-            dma((2,)),
+            dma((seqs // 8,)),
             dma,
             dma((n_tp - 1,)),
             dma,
@@ -814,6 +859,7 @@
             dma((n_tp,)),
             dma,
             dma((n_tp,)),
+            pltpu.SemaphoreType.REGULAR((n_ep // 2 - 1, 2)),
             *[vmem(each.shape, each.dtype) for each in small],
             dma((len(small),)),
         ],

time: 33.7 us -> 31.1 us (0.923)
  Pallas kernels: 32.9 us -> 30.3 us
    pallas_call x1, Pallas kernels: 32.9 us -> 30.3 us  [local(): pl.pallas_call(functools.partial(layer_entry, n_ep, n_tp, slots, len(smal...]
where the time goes in v2:
time: 31.1 us; the launch traced here: 31 us
  Pallas kernels  30.3 us (97%)
  local copies, waits for them, and re-layouts  0.62 us (2%)
    pallas_call x1, Pallas kernels, local(): pl.pallas_call(functools.partial(layer_entry, n_ep, n_tp, slots, len(smal...  30.3 us
    unnamed x1, local copies, waits for them, and re-layouts  0.62 us

profile of v2, /device:TPU:0, one launch (start us, length us, event | category | flops | bytes accessed | tf_op | source)
XLA Modules:
  0.0 31.0 jit_solution(7521297469571255497)
XLA Ops:
  0.0 30.3 %layer.1 = bf16[48,512]{1,0:T(8,128)(2,1)S(1)} custom-call(bf16[48,512]{1,0:T(8,128)(2,1)} %refs_0_.1, f32[1,2048]{1,0:T(1,128)} %bitcast.24, f32[1,32]{1,0:T(1,128)} %bitcast.29, f32[1,32]{1,0:T(1,128)} %bitcast.30, f32[1,32]{1,0:T(1,128)} %bitcast.31, bf16[4,512]{1,0:T(4,128)(2,1)} %refs_5_.1, bf16[4,256]{1,0:T(4,128)(2,1)} %refs_6_.1, ...), custom_call_target="tpu_custom_call" | custom-call | tf_op jit(solution)/shard_map/layer/pallas_call | solution.py:818
  30.3 0.6 %copy.27 = bf16[48,512]{1,0:T(8,128)(2,1)} copy(bf16[48,512]{1,0:T(8,128)(2,1)S(1)} %layer.1) | data formatting | bytes 98304

commit v3 on v2

--- a/solution.py
+++ b/solution.py
@@ -160,6 +160,7 @@
 LANES = 128
 TILE = 256
 ROW_SEND, ROW_USE = (0, 1, 2, 3), (0, 1, 2, 3)
+STATE_BLOCKS = 2
 
 
 def silu(v):
@@ -256,7 +257,8 @@
     exp_down,
     gathered,
     normed,
-    queries,
+    raw_value,
+    raw_gate,
     state_read,
     mix_send,
     mix_recv,
@@ -536,31 +538,48 @@
     wide = dot32(jnp.concatenate([spread_high, spread_low], axis=0), spread)
     step_wide = wide[0:seqs] + wide[2 * seqs : 3 * seqs]
     decay_wide = wide[seqs : 2 * seqs] + wide[3 * seqs : 4 * seqs]
-    mark("value")
-    values = silu(past_x + dot32(normed[...], w_value_x[...]) * taps_x[last : last + 1, :])
-    direct = values * (step_wide * key_query + skip)
-    gate_z = silu(dot32(normed[...], w_gate_z[...]))
+    asked = jnp.concatenate([query, jnp.zeros((LANES - seqs, STATE), F32)], axis=0).T
+    lane_seq = lax.broadcasted_iota(jnp.int32, (STATE, LANES), 1)
+    state_read[...] = jnp.zeros(state_read.shape, F32)
+    part_cols = width // state_blocks
 
     mark("state")
-
-    queries[...] = query
-    turn_on(2, turns)
 
     def read_block(block, carry):
         load_state(block).wait()
-        rows = pl.ds(pl.multiple_of(block * 8, 8), 8)
-        asked = queries[rows, :].astype(BF)
-        row_of = lax.broadcasted_iota(jnp.int32, (8, width), 0)
-        total_read = jnp.zeros((8, width), F32)
-        for row in range(8):
-            held = state[block * 8 + row].astype(BF)
-            total_read = jnp.where(row_of == row, dot32_t(asked, held), total_read)
-        state_read[rows, :] = total_read
+
+        @pl.when(block == state_blocks - 1)
+        def _():
+            turn_on(2, turns)
+
+        columns = pl.ds(pl.multiple_of(block * part_cols, LANES), part_cols)
+        raw_value[:, columns] = dot32(normed[...], w_value_x[:, columns])
+        raw_gate[:, columns] = dot32(normed[...], w_gate_z[:, columns])
+        found = None
+        for pair in range(state_rows // 2):
+            first = block * state_rows + pair * 2
+            held = jnp.concatenate([state[first], state[first + 1]], axis=1).astype(BF)
+            wanted = jnp.concatenate(
+                [
+                    jnp.where(lane_seq == first, asked, 0.0),
+                    jnp.where(lane_seq == first + 1, asked, 0.0),
+                ],
+                axis=0,
+            ).astype(BF)
+            part = dot32(held, wanted)
+            found = part if found is None else found + part
+        state_read[...] = state_read[...] + found
         return carry
 
-    lax.fori_loop(0, seqs // 8, read_block, 0)
+    lax.fori_loop(0, state_blocks, read_block, 0)
+    mark("values")
+    found = state_read[...].T[0:seqs, :]
+    values = silu(past_x + raw_value[...] * taps_x[last : last + 1, :])
+    direct = values * (step_wide * key_query + skip)
+    gate_z = silu(raw_gate[...])
+
     mark("gated")
-    gated = (decay_wide * state_read[...] + direct) * gate_z
+    gated = (decay_wide * found + direct) * gate_z
     squared = gated * gated
     squared = jnp.concatenate(
         [squared[:, tile * LANES : (tile + 1) * LANES] for tile in range(tiles)], axis=0
@@ -774,7 +793,10 @@
         or route_ids.shape[1] != 2
         or width % LANES
         or units % TILE
+        or seqs % (2 * STATE_BLOCKS)
         or seqs % 16
+        or seqs > LANES
+        or width % (LANES * STATE_BLOCKS)
         or n_ep * slots * (width // LANES) % 16
         or n_ep % 2
         or n_ep < 4
@@ -833,8 +855,9 @@
             vmem(expert_down.shape[1:], BF),
             vmem((n_tp - 1, seqs, width), BF),
             vmem((seqs, features), BF),
-            vmem((seqs, STATE), F32),
             vmem((seqs, width), F32),
+            vmem((seqs, width), F32),
+            vmem((width, LANES), F32),
             vmem((n_tp - 1, seqs, width), BF),
             vmem((n_tp - 1, seqs, width), BF),
             vmem(exchange, BF),
@@ -850,7 +873,7 @@
             vmem(exchange, BF),
             vmem(exchange, BF),
             dma((9,)),
-            dma((seqs // 8,)),
+            dma((STATE_BLOCKS,)),
             dma,
             dma((n_tp - 1,)),
             dma,

time: 31.1 us -> 30.8 us (level)
  no operation moved by 1% of the time
where the time goes in v3:
time: 30.8 us; the launch traced here: 30.7 us
  Pallas kernels  30 us (97%)
  local copies, waits for them, and re-layouts  0.62 us (2%)
    pallas_call x1, Pallas kernels, local(): pl.pallas_call(functools.partial(layer_entry, n_ep, n_tp, slots, len(smal...  30 us
    unnamed x1, local copies, waits for them, and re-layouts  0.62 us

profile of v3, /device:TPU:0, one launch (start us, length us, event | category | flops | bytes accessed | tf_op | source)
XLA Modules:
  0.0 30.7 jit_solution(18252317796072970260)
XLA Ops:
  0.0 30.0 %layer.1 = bf16[48,512]{1,0:T(8,128)(2,1)S(1)} custom-call(bf16[48,512]{1,0:T(8,128)(2,1)} %refs_0_.1, f32[1,2048]{1,0:T(1,128)} %bitcast.24, f32[1,32]{1,0:T(1,128)} %bitcast.29, f32[1,32]{1,0:T(1,128)} %bitcast.30, f32[1,32]{1,0:T(1,128)} %bitcast.31, bf16[4,512]{1,0:T(4,128)(2,1)} %refs_5_.1, bf16[4,256]{1,0:T(4,128)(2,1)} %refs_6_.1, ...), custom_call_target="tpu_custom_call" | custom-call | tf_op jit(solution)/shard_map/layer/pallas_call | solution.py:840
  30.0 0.6 %copy.27 = bf16[48,512]{1,0:T(8,128)(2,1)} copy(bf16[48,512]{1,0:T(8,128)(2,1)S(1)} %layer.1) | data formatting | bytes 98304

commit v4 on v3

--- a/solution.py
+++ b/solution.py
@@ -161,6 +161,7 @@
 TILE = 256
 ROW_SEND, ROW_USE = (0, 1, 2, 3), (0, 1, 2, 3)
 STATE_BLOCKS = 2
+GATE_EARLY = 0
 
 
 def silu(v):
@@ -258,7 +259,6 @@
     gathered,
     normed,
     raw_value,
-    raw_gate,
     state_read,
     mix_send,
     mix_recv,
@@ -380,10 +380,11 @@
                 chain_send(turn)
 
     mark("loads")
-    for each in (load_query, load_key, load_step, load_value, load_gate):
+    for each in (load_query, load_key, load_step, load_value):
         each.start()
     for block in range(state_blocks):
-        load_state(block).start(priority=1)
+        load_state(block).start(priority=GATE_EARLY)
+    load_gate.start(priority=1)
     mark("smallwait")
     fetches[0].wait()
     mark("barrier")
@@ -525,7 +526,7 @@
         normed[:, columns] = (piece.astype(F32) * scale * mix_gain[:, columns]).astype(BF)
     turn_on(1, 2)
     mark("projwait")
-    for each in (load_query, load_key, load_step, load_value, load_gate):
+    for each in (load_query, load_key, load_step, load_value):
         each.wait()
     mark("query")
     query = silu(past_c + dot32(normed[...], w_query_c[...]) * taps_c[last : last + 1, :])
@@ -554,7 +555,6 @@
 
         columns = pl.ds(pl.multiple_of(block * part_cols, LANES), part_cols)
         raw_value[:, columns] = dot32(normed[...], w_value_x[:, columns])
-        raw_gate[:, columns] = dot32(normed[...], w_gate_z[:, columns])
         found = None
         for pair in range(state_rows // 2):
             first = block * state_rows + pair * 2
@@ -573,10 +573,11 @@
 
     lax.fori_loop(0, state_blocks, read_block, 0)
     mark("values")
+    load_gate.wait()
+    gate_z = silu(dot32(normed[...], w_gate_z[...]))
     found = state_read[...].T[0:seqs, :]
     values = silu(past_x + raw_value[...] * taps_x[last : last + 1, :])
     direct = values * (step_wide * key_query + skip)
-    gate_z = silu(raw_gate[...])
 
     mark("gated")
     gated = (decay_wide * found + direct) * gate_z
@@ -856,7 +857,6 @@
             vmem((n_tp - 1, seqs, width), BF),
             vmem((seqs, features), BF),
             vmem((seqs, width), F32),
-            vmem((seqs, width), F32),
             vmem((width, LANES), F32),
             vmem((n_tp - 1, seqs, width), BF),
             vmem((n_tp - 1, seqs, width), BF),

time: 30.8 us -> 30.8 us (level)
  no operation moved by 1% of the time
where the time goes in v4:
time: 30.8 us; the launch traced here: 30.7 us
  Pallas kernels  30 us (97%)
  local copies, waits for them, and re-layouts  0.62 us (2%)
    pallas_call x1, Pallas kernels, local(): pl.pallas_call(functools.partial(layer_entry, n_ep, n_tp, slots, len(smal...  30 us
    unnamed x1, local copies, waits for them, and re-layouts  0.62 us

profile of v4, /device:TPU:0, one launch (start us, length us, event | category | flops | bytes accessed | tf_op | source)
XLA Modules:
  0.0 30.7 jit_solution(7915188057487531157)
XLA Ops:
  0.0 30.0 %layer.1 = bf16[48,512]{1,0:T(8,128)(2,1)S(1)} custom-call(bf16[48,512]{1,0:T(8,128)(2,1)} %refs_0_.1, f32[1,2048]{1,0:T(1,128)} %bitcast.24, f32[1,32]{1,0:T(1,128)} %bitcast.29, f32[1,32]{1,0:T(1,128)} %bitcast.30, f32[1,32]{1,0:T(1,128)} %bitcast.31, bf16[4,512]{1,0:T(4,128)(2,1)} %refs_5_.1, bf16[4,256]{1,0:T(4,128)(2,1)} %refs_6_.1, ...), custom_call_target="tpu_custom_call" | custom-call | tf_op jit(solution)/shard_map/layer/pallas_call | solution.py:841
  30.0 0.6 %copy.27 = bf16[48,512]{1,0:T(8,128)(2,1)} copy(bf16[48,512]{1,0:T(8,128)(2,1)S(1)} %layer.1) | data formatting | bytes 98304
